TPU v7x, 32 devices: a whole 2x2x4 slice. The times are simulated.
32 devices in a mesh: ep: 4 (over y, x), tp: 8 (over z, core).
Axes of the slice: x: 2, y: 2, z: 4, core: 2. Of those that a mesh axis runs over, the one named last changes fastest.
Arguments:
- tokens: bfloat16 [1024, 1024], P(('ep', 'tp')), may hold values from -6 to 6
- norm_gain: float32 [1024], replicated, may hold values from 0.5 to 1.5
- routing: int32 [1024, 2], P('ep'), may hold values from 0 to 7, as said below
- gate_share: float32 [1024, 2], P('ep'), may hold values from 0.5 to 1.5
- w_gate: bfloat16 [8, 1024, 256], P('ep', None, 'tp'), may hold values from -0.1875 to 0.1875
- w_up: bfloat16 [8, 1024, 256], P('ep', None, 'tp'), may hold values from -0.1875 to 0.1875
- w_down: bfloat16 [8, 256, 1024], P('ep', 'tp'), may hold values from -0.375 to 0.375
Outputs:
- mixed_out: bfloat16 [1024, 1024], P('ep', 'tp')
Inputs may be any that keep to these rules, and one draw needn't show every extreme that they name: `routing`: each row names two different experts whose ids lie in the same block of 2 consecutive ids. In each aligned block of 256 rows (the tokens of one index of ep) no expert is named by more than 128 rows, and some expert is named by exactly 128.
All inputs are finite; a program needn't handle non-finite values.
Results may differ from a plain program's by a relative error of at most 0.0015.
Values may be sent and summed in bfloat16 or wider, within the bound.
A program may use at most 64 MiB of HBM per device.

v0:
```python
import jax
import jax.numpy as jnp
from jax import lax
from jax.sharding import PartitionSpec as P

epsilon = 1e-06


def norm_rows(tokens, norm_gain):
    as_float = tokens.astype(jnp.float32)
    scaled = as_float * lax.rsqrt(jnp.mean(as_float * as_float, axis=-1, keepdims=True) + epsilon)
    return (scaled * norm_gain.astype(jnp.float32)).astype(jnp.bfloat16)


def fill_buffer(group, flat_target, slots, model_width):
    buffer = jnp.zeros((slots, model_width), jnp.bfloat16)
    return buffer.at[flat_target].set(jnp.repeat(group, 2, axis=0))


def body(tokens, norm_gain, routing, gate_share, w_gate, w_up, w_down):
    ep_size = lax.axis_size("ep")
    tp_size = lax.axis_size("tp")
    local_experts = w_gate.shape[0]
    experts = local_experts * ep_size
    group_rows = routing.shape[0]
    capacity = group_rows * 4 // experts
    model_width = tokens.shape[1]
    columns = model_width // tp_size
    normed = norm_rows(tokens, norm_gain)
    onehot = (routing[:, :, None] == jnp.arange(experts, dtype=jnp.int32)[None, None, :]).astype(
        jnp.int32
    )
    flat_hot = onehot.reshape(group_rows * 2, experts)
    ranking = jnp.cumsum(flat_hot, axis=0) - 1
    slot_pos = jnp.sum(ranking * flat_hot, axis=1).reshape(group_rows, 2)
    target = (routing * capacity + slot_pos).astype(jnp.int32)
    flat_target = target.reshape(-1)
    slice_len = capacity // tp_size
    tp_index = lax.axis_index("tp")
    group = lax.all_gather(normed, "tp", axis=0, tiled=True)
    buffer = fill_buffer(group, flat_target, experts * capacity, model_width)
    shaped = buffer.reshape(ep_size, local_experts, capacity, model_width)
    mine = lax.dynamic_slice_in_dim(shaped, tp_index * slice_len, slice_len, 2)
    mine = mine.reshape(ep_size, local_experts * slice_len, model_width)
    landed = lax.all_to_all(mine, "ep", split_axis=0, concat_axis=0, tiled=True)
    landed = landed.reshape(ep_size, local_experts, slice_len, model_width).transpose(1, 0, 2, 3)
    landed = landed.reshape(local_experts, ep_size * slice_len, model_width)
    full_gate, full_up, full_down = (
        lax.all_gather(w_gate, "tp", axis=2, tiled=True),
        lax.all_gather(w_up, "tp", axis=2, tiled=True),
        lax.all_gather(w_down, "tp", axis=1, tiled=True),
    )
    gate_sum = jnp.einsum("erd,edh->erh", landed, full_gate, preferred_element_type=jnp.float32)
    up_sum = jnp.einsum("erd,edh->erh", landed, full_up, preferred_element_type=jnp.float32)
    hidden = (jax.nn.silu(gate_sum) * up_sum).astype(jnp.bfloat16)
    produced = jnp.einsum(
        "erh,ehd->erd", hidden, full_down, preferred_element_type=jnp.float32
    ).astype(jnp.bfloat16)
    produced = produced.reshape(local_experts, ep_size, slice_len, model_width)
    blocks = lax.all_to_all(produced, "tp", split_axis=3, concat_axis=2, tiled=True)
    leaving = blocks.transpose(1, 0, 2, 3).reshape(ep_size, local_experts * capacity, columns)
    returned = lax.all_to_all(leaving, "ep", split_axis=0, concat_axis=0, tiled=True).reshape(
        experts * capacity, columns
    )
    picked_out = returned[target]
    mixed_out = jnp.sum(gate_share[:, :, None] * picked_out.astype(jnp.float32), axis=1)
    return mixed_out.astype(jnp.bfloat16)


def solution(mesh):
    return jax.shard_map(
        body,
        mesh=mesh,
        in_specs=(
            P(("ep", "tp"), None),
            P(),
            P("ep", None),
            P("ep", None),
            P("ep", None, "tp"),
            P("ep", None, "tp"),
            P("ep", "tp", None),
        ),
        out_specs=P("ep", "tp"),
        check_vma=False,
    )
```

profile of v0, /device:TPU:0, one launch (start us, length us, event | category | flops | bytes accessed | tf_op | source)
XLA Modules:
  0.0 124.2 jit_solution(3098279486913121579)
XLA Ops:
  6.5 0.7 all-gather.4.cloned.1.call-update
  7.3 0.7 all-gather.6.cloned.1.call-update
  8.1 0.7 all-gather.8.cloned.1.call-update
  8.7 0.8 copy.34
  9.6 0.1 eq.30
  9.7 0.1 eq.26
  9.9 1.1 reduce-window.6
  11.0 0.2 slice_reduce_fusion
  11.4 0.1 reshape.89
  11.6 0.7 compare_select_fusion.1
  12.4 0.2 reshape.90
  12.6 1.0 fusion.4
  13.6 0.9 fusion.6
  14.5 19.1 %all_gather.12 = bf16[256,1024]{1,0:T(8,128)(2,1)S(1)} all-gather(bf16[32,1024]{1,0:T(8,128)(2,1)S(1)} %fusion.6), channel_id=1, replica_groups=mesh['ep'=4,'tp'=8] {'tp'}, dimensions={0}, use_global_device_ids=true | all-gather | bytes 589824 | tf_op jit(solution)/shard_map/all_gather | solution.py:40
  33.6 0.5 broadcast_in_dim.7
  34.2 0.4 reshape.111
  34.6 3.2 %scatter_custom_fusion = bf16[1024,1024]{1,0:T(8,128)(2,1)S(1)} fusion(s32[512]{0:T(512)S(1)} %bitcast.42, bf16[512,1024]{1,0:T(8,128)(2,1)S(1)} %reshape.111, bf16[]{:T(256)} %constant.11.clone.1), kind=kCustom, calls=%fused_computation.5 | custom fusion | bytes 2097154 | tf_op jit(solution)/shard_map/scatter | solution.py:17
  37.9 9.8 %all_to_all.28 = bf16[4,32,1024]{2,1,0:T(8,128)(2,1)S(1)} all-to-all(bf16[4,32,1024]{2,1,0:T(8,128)(2,1)S(1)} %bitcast.38), channel_id=1, replica_groups=mesh['ep'=4,'tp'=8] {'ep'}, dimensions={0} | all-to-all | bytes 524288 | tf_op jit(solution)/shard_map/all_to_all | solution.py:45
  47.7 1.7 %fusion.16 = f32[2,64,256]{2,1,0:T(8,128)S(1)} fusion(bf16[2,64,1024]{2,1,0:T(8,128)(2,1)S(1)} %bitcast.36, bf16[2,1024,256]{1,2,0:T(8,128)(2,1)} %all-gather.4.cloned.1.call-done), kind=kOutput, calls=%fused_computation.33 | convolution fusion | flops 67108864 | bytes 1441792 | tf_op jit(solution)/shard_map/erd,edh->erh/dot_general | solution.py:53
  49.4 10.8 %all-gather.6.cloned.1.call-done = bf16[2,1024,256]{1,2,0:T(8,128)(2,1)} async-done(((bf16[2,1024,32]{1,2,0:T(8,128)(2,1)}), bf16[2,1024,256]{1,2,0:T(8,128)(2,1)}) %all-gather.6.cloned.1.call-update) | async-done | bytes 1048592 | tf_op jit(solution)/shard_map/all_gather | solution.py:50
  60.2 23.5 %all-gather.8.cloned.1.call-done = bf16[2,256,1024]{2,1,0:T(8,128)(2,1)} async-done(((bf16[2,32,1024]{2,1,0:T(8,128)(2,1)}), bf16[2,256,1024]{2,1,0:T(8,128)(2,1)}) %all-gather.8.cloned.1.call-update) | async-done | bytes 1048592 | tf_op jit(solution)/shard_map/all_gather | solution.py:51
  83.7 2.2 %convolution_convert_fusion = bf16[2,64,1024]{2,1,0:T(8,128)(2,1)S(1)} fusion(bf16[2,256,1024]{2,1,0:T(8,128)(2,1)} %all-gather.8.cloned.1.call-done, bf16[2,64,1024]{2,1,0:T(8,128)(2,1)S(1)} %bitcast.37, bf16[2,1024,256]{1,2,0:T(8,128)(2,1)} %all-gather.6.cloned.1.call-done, f32[2,64,256]{2,1,0:T(8,128)S(1)} %fusion.16), kind=kOutput, calls=%fused_computation.2 | convolution fusion | flops 134545408 | bytes 2752512 | tf_op jit(solution)/shard_map/erh,ehd->erd/dot_general | solution.py:56
  85.9 1.4 %copy.39 = bf16[2,4,16,1024]{2,1,0,3:T(4,128)(2,1)S(1)} copy(bf16[2,4,16,1024]{3,2,1,0:T(8,128)(2,1)S(1)} %bitcast.40) | data formatting | bytes 524288 | tf_op jit(solution)/shard_map/reshape | solution.py:59
  87.3 2.2 %reshape.121 = bf16[8,2,8192]{2,1,0:T(2,128)(2,1)S(1)} reshape(bf16[1024,2,4,16]{3,2,1,0:T(4,128)(2,1)S(1)} %bitcast.32) | data formatting | bytes 524288
  89.5 12.9 %all_to_all.29 = bf16[8,2,8192]{2,1,0:T(2,128)(2,1)S(1)} all-to-all(bf16[8,2,8192]{2,1,0:T(2,128)(2,1)S(1)} %reshape.121), channel_id=1, replica_groups=mesh['ep'=4,'tp'=8] {'tp'}, dimensions={0} | all-to-all | bytes 524288 | tf_op jit(solution)/shard_map/all_to_all | solution.py:60
  102.3 1.4 %reshape.122 = bf16[1024,2,4,16]{3,2,1,0:T(4,128)(2,1)S(1)} reshape(bf16[8,2,8192]{2,1,0:T(2,128)(2,1)S(1)} %all_to_all.29) | data formatting | bytes 524288
  103.8 2.6 %copy.46 = bf16[2,4,16,8,128]{4,2,3,0,1:T(8,128)(2,1)} copy(bf16[2,4,16,8,128]{2,1,0,4,3:T(4,128)(2,1)S(1)} %bitcast.33) | data formatting | bytes 524288 | tf_op jit(solution)/shard_map/transpose | solution.py:61
  106.4 3.6 %all-to-all-start.2 = ((bf16[4,256,128]{2,1,0:T(8,128)(2,1)}), bf16[4,256,128]{2,1,0:T(8,128)(2,1)S(1)}, u32[]{:S(2)}, u32[]{:S(2)}) async-start(bf16[4,256,128]{2,1,0:T(8,128)(2,1)} %bitcast.15), calls=%async_computation.2 | async-start | bytes 524288 | tf_op jit(solution)/shard_map/all_to_all | solution.py:62
  110.1 0.1 reshape.101
  110.4 4.9 %all-to-all-done.2 = bf16[4,256,128]{2,1,0:T(8,128)(2,1)S(1)} async-done(((bf16[4,256,128]{2,1,0:T(8,128)(2,1)}), bf16[4,256,128]{2,1,0:T(8,128)(2,1)S(1)}, u32[]{:S(2)}, u32[]{:S(2)}) %all-to-all-start.2) | async-done | bytes 262176 | tf_op jit(solution)/shard_map/all_to_all | solution.py:62
  115.3 1.3 %gather_fusion = bf16[512,128]{1,0:T(8,128)(2,1)S(1)} fusion(bf16[1024,128]{1,0:T(8,128)(2,1)S(1)} %bitcast.34, s32[1024]{0:T(1024)S(1)} %pad_clamp_fusion), kind=kCustom, calls=%fused_computation | custom fusion | bytes 264192 | tf_op jit(solution)/shard_map/gather | solution.py:65
  116.7 1.1 fusion.3
  (19 shorter events, 0.8 us)
Async XLA Ops:
  6.5 41.2 %all-gather.4.cloned.1.call-start = ((), (), s32[]{:S(2)}) async-start(), calls=%async_computation.3 | async-start | bytes 1179648 | tf_op jit(solution)/shard_map/all_gather | solution.py:49
  7.3 52.9 %all-gather.6.cloned.1.call-start = ((), (), s32[]{:S(2)}) async-start(), calls=%async_computation.4 | async-start | bytes 1179648 | tf_op jit(solution)/shard_map/all_gather | solution.py:50
  8.0 75.7 %all-gather.8.cloned.1.call-start = ((), (), s32[]{:S(2)}) async-start(), calls=%async_computation.5 | async-start | bytes 1179648 | tf_op jit(solution)/shard_map/all_gather | solution.py:51
  103.8 6.5 %copy-start = (f32[256,2]{0,1:T(2,128)S(1)}, f32[256,2]{0,1:T(2,128)}, u32[]{:S(2)}) copy-start(f32[256,2]{0,1:T(2,128)} %param.10) | copy-start | bytes 6148
  106.4 9.0 %all-to-all-start.2 = ((bf16[4,256,128]{2,1,0:T(8,128)(2,1)}), bf16[4,256,128]{2,1,0:T(8,128)(2,1)S(1)}, u32[]{:S(2)}, u32[]{:S(2)}) async-start(bf16[4,256,128]{2,1,0:T(8,128)(2,1)} %bitcast.15), calls=%async_computation.2 | async-start | bytes 524288 | tf_op jit(solution)/shard_map/all_to_all | solution.py:62
Sparse Core Ops, SparseCore 0:
  8.9 27.6 all-gather.3
  38.3 21.8 all-gather.5
  61.8 21.8 all-gather.7
where the time goes:
time: 125 us; the launch traced here: 124 us
  blocking collectives  41.8 us (33%)
  waiting for transfers between devices  41.3 us (33%)
  local copies, waits for them, and re-layouts  15.3 us (12%)
  between operations  13.3 us (11%)
  other arithmetic  4.95 us (4%)
  matrix products  3.9 us (3%)
  starting transfers between devices  3.66 us (3%)
    all_gather x1, waiting for transfers between devices, body(): lax.all_gather(w_down, 'tp', axis=1, tiled=True)  23.5 us
    all_gather x1, blocking collectives, body(): group = lax.all_gather(normed, 'tp', axis=0, tiled=True)  19.1 us
    all_to_all x1, blocking collectives, body(): lax.all_to_all(produced, 'tp', split_axis=3, concat_axis=2, tiled=True)  12.9 us
    all_gather x1, waiting for transfers between devices, body(): lax.all_gather(w_up, 'tp', axis=2, tiled=True)  10.8 us
    all_to_all x1, blocking collectives, body(): landed = lax.all_to_all(mine, 'ep', split_axis=0, concat_axis=0, tiled=True)  9.78 us
    all_to_all x1, waiting for transfers between devices, body(): lax.all_to_all(leaving, 'ep', split_axis=0, concat_axis=0, tiled=True)  4.92 us
    unnamed x6, local copies, waits for them, and re-layouts  4.55 us
    all_to_all x1, starting transfers between devices, body(): lax.all_to_all(leaving, 'ep', split_axis=0, concat_axis=0, tiled=True)  3.58 us
  transfers between devices with their start and end apart: 4, of which 3 were waited for; matrix products, arithmetic and copies ran while one was open for 10% of the time, Pallas kernels for 0%

commit v1 on v0

--- a/solution.py
+++ b/solution.py
@@ -57,7 +57,10 @@
         "erh,ehd->erd", hidden, full_down, preferred_element_type=jnp.float32
     ).astype(jnp.bfloat16)
     produced = produced.reshape(local_experts, ep_size, slice_len, model_width)
-    blocks = lax.all_to_all(produced, "tp", split_axis=3, concat_axis=2, tiled=True)
+    blocks = jnp.concatenate(
+        lax.all_to_all(jnp.stack(jnp.split(produced, lax.axis_size("tp"), axis=3)), "tp", 0, 0),
+        axis=2,
+    )
     leaving = blocks.transpose(1, 0, 2, 3).reshape(ep_size, local_experts * capacity, columns)
     returned = lax.all_to_all(leaving, "ep", split_axis=0, concat_axis=0, tiled=True).reshape(
         experts * capacity, columns

time: 125 us -> 118 us (0.944)
  local copies, waits for them, and re-layouts: 15.3 us -> 8.68 us
    unnamed x6 -> x11, local copies, waits for them, and re-layouts: 4.55 us -> 1.07 us
    transpose x1, local copies, waits for them, and re-layouts: 2.57 us -> 0.71 us  [body(): blocks.transpose(1, 0, 2, 3)]
    reshape x1 -> x0, local copies, waits for them, and re-layouts: 1.36 us -> none  [body(): produced = produced.reshape(local_experts, ep_size, slice_len, model_width)]
where the time goes in v1:
time: 118 us
  blocking collectives  41.8 us (35%)
  waiting for transfers between devices  41.3 us (35%)
  between operations  13.3 us (11%)
  local copies, waits for them, and re-layouts  8.68 us (7%)
  other arithmetic  4.95 us (4%)
  matrix products  3.9 us (3%)
  starting transfers between devices  3.66 us (3%)
    all_gather x1, waiting for transfers between devices, body(): lax.all_gather(w_down, 'tp', axis=1, tiled=True)  23.5 us
    all_gather x1, blocking collectives, body(): group = lax.all_gather(normed, 'tp', axis=0, tiled=True)  19.1 us
    all_to_all x1, blocking collectives, body(): lax.all_to_all(jnp.stack(jnp.split(produced, lax.axis_size('tp'), axis=3)...  12.9 us
    all_gather x1, waiting for transfers between devices, body(): lax.all_gather(w_up, 'tp', axis=2, tiled=True)  10.8 us
    all_to_all x1, blocking collectives, body(): landed = lax.all_to_all(mine, 'ep', split_axis=0, concat_axis=0, tiled=True)  9.78 us
    all_to_all x1, waiting for transfers between devices, body(): lax.all_to_all(leaving, 'ep', split_axis=0, concat_axis=0, tiled=True)  4.92 us
    all_to_all x1, starting transfers between devices, body(): lax.all_to_all(leaving, 'ep', split_axis=0, concat_axis=0, tiled=True)  3.58 us
    scatter x1, local copies, waits for them, and re-layouts, fill_buffer(): return buffer.at[flat_target].set(jnp.repeat(group, 2, axis=0))  3.23 us
  transfers between devices with their start and end apart: 4, of which 3 were waited for; matrix products, arithmetic and copies ran while one was open for 10% of the time, Pallas kernels for 0%

profile of v1, /device:TPU:0, one launch (start us, length us, event | category | flops | bytes accessed | tf_op | source)
XLA Modules:
  0.0 117.6 jit_solution(18286929020865902042)
XLA Ops:
  6.5 0.7 all-gather.4.cloned.1.call-update
  7.3 0.7 all-gather.6.cloned.1.call-update
  8.1 0.7 all-gather.8.cloned.1.call-update
  8.7 0.8 copy.45
  9.6 0.1 eq.30
  9.7 0.1 eq.26
  9.9 1.1 reduce-window.6
  11.0 0.2 slice_reduce_fusion
  11.4 0.1 reshape.95
  11.6 0.7 compare_select_fusion.1
  12.3 0.1 copy.48
  12.4 0.2 reshape.96
  12.6 1.0 fusion.4
  13.6 0.9 fusion.6
  14.5 19.1 %all_gather.12 = bf16[256,1024]{1,0:T(8,128)(2,1)S(1)} all-gather(bf16[32,1024]{1,0:T(8,128)(2,1)S(1)} %fusion.6), channel_id=1, replica_groups=mesh['ep'=4,'tp'=8] {'tp'}, dimensions={0}, use_global_device_ids=true | all-gather | bytes 589824 | tf_op jit(solution)/shard_map/all_gather | solution.py:40
  33.6 0.5 broadcast_in_dim.7
  34.2 0.4 reshape.119
  34.6 3.2 %scatter_custom_fusion = bf16[1024,1024]{1,0:T(8,128)(2,1)S(1)} fusion(s32[512]{0:T(512)S(1)} %bitcast.76, bf16[512,1024]{1,0:T(8,128)(2,1)S(1)} %reshape.119, bf16[]{:T(256)} %constant.11.clone.1), kind=kCustom, calls=%fused_computation.5 | custom fusion | bytes 2097154 | tf_op jit(solution)/shard_map/scatter | solution.py:17
  37.9 9.8 %all_to_all.15 = bf16[4,32,1024]{2,1,0:T(8,128)(2,1)S(1)} all-to-all(bf16[4,32,1024]{2,1,0:T(8,128)(2,1)S(1)} %bitcast.64), channel_id=1, replica_groups=mesh['ep'=4,'tp'=8] {'ep'}, dimensions={0} | all-to-all | bytes 524288 | tf_op jit(solution)/shard_map/all_to_all | solution.py:45
  47.7 1.7 %fusion.24 = f32[2,64,256]{2,1,0:T(8,128)S(1)} fusion(bf16[2,64,1024]{2,1,0:T(8,128)(2,1)S(1)} %bitcast.62, bf16[2,1024,256]{1,2,0:T(8,128)(2,1)} %all-gather.4.cloned.1.call-done), kind=kOutput, calls=%fused_computation.49 | convolution fusion | flops 67108864 | bytes 1441792 | tf_op jit(solution)/shard_map/erd,edh->erh/dot_general | solution.py:53
  49.4 10.8 %all-gather.6.cloned.1.call-done = bf16[2,1024,256]{1,2,0:T(8,128)(2,1)} async-done(((bf16[2,1024,32]{1,2,0:T(8,128)(2,1)}), bf16[2,1024,256]{1,2,0:T(8,128)(2,1)}) %all-gather.6.cloned.1.call-update) | async-done | bytes 1048592 | tf_op jit(solution)/shard_map/all_gather | solution.py:50
  60.2 23.5 %all-gather.8.cloned.1.call-done = bf16[2,256,1024]{2,1,0:T(8,128)(2,1)} async-done(((bf16[2,32,1024]{2,1,0:T(8,128)(2,1)}), bf16[2,256,1024]{2,1,0:T(8,128)(2,1)}) %all-gather.8.cloned.1.call-update) | async-done | bytes 1048592 | tf_op jit(solution)/shard_map/all_gather | solution.py:51
  83.7 2.2 %convolution_convert_fusion = bf16[2,64,1024]{2,1,0:T(8,128)(2,1)S(1)} fusion(bf16[2,256,1024]{2,1,0:T(8,128)(2,1)} %all-gather.8.cloned.1.call-done, bf16[2,64,1024]{2,1,0:T(8,128)(2,1)S(1)} %bitcast.63, bf16[2,1024,256]{1,2,0:T(8,128)(2,1)} %all-gather.6.cloned.1.call-done, f32[2,64,256]{2,1,0:T(8,128)S(1)} %fusion.24), kind=kOutput, calls=%fused_computation.2 | convolution fusion | flops 134545408 | bytes 2752512 | tf_op jit(solution)/shard_map/erh,ehd->erd/dot_general | solution.py:56
  86.1 12.9 %all_to_all.16 = bf16[8,2,4,16,128]{4,3,2,1,0:T(8,128)(2,1)S(1)} all-to-all(bf16[8,2,4,16,128]{4,3,2,1,0:T(8,128)(2,1)S(1)} %fusion.13), channel_id=1, replica_groups=mesh['ep'=4,'tp'=8] {'tp'}, dimensions={0} | all-to-all | bytes 524288 | tf_op jit(solution)/shard_map/all_to_all | solution.py:61
  99.0 0.7 copy.51
  99.7 3.6 %all-to-all-start.2 = ((bf16[4,256,128]{2,1,0:T(8,128)(2,1)}), bf16[4,256,128]{2,1,0:T(8,128)(2,1)S(1)}, u32[]{:S(2)}, u32[]{:S(2)}) async-start(bf16[4,256,128]{2,1,0:T(8,128)(2,1)} %bitcast.20), calls=%async_computation.2 | async-start | bytes 524288 | tf_op jit(solution)/shard_map/all_to_all | solution.py:65
  103.3 0.1 copy.52
  103.4 0.1 reshape.109
  103.6 0.1 copy.44
  103.8 4.9 %all-to-all-done.2 = bf16[4,256,128]{2,1,0:T(8,128)(2,1)S(1)} async-done(((bf16[4,256,128]{2,1,0:T(8,128)(2,1)}), bf16[4,256,128]{2,1,0:T(8,128)(2,1)S(1)}, u32[]{:S(2)}, u32[]{:S(2)}) %all-to-all-start.2) | async-done | bytes 262176 | tf_op jit(solution)/shard_map/all_to_all | solution.py:65
  108.7 1.3 %gather_fusion = bf16[512,128]{1,0:T(8,128)(2,1)S(1)} fusion(bf16[1024,128]{1,0:T(8,128)(2,1)S(1)} %bitcast.60, s32[1024]{0:T(1024)S(1)} %pad_clamp_fusion), kind=kCustom, calls=%fused_computation | custom fusion | bytes 264192 | tf_op jit(solution)/shard_map/gather | solution.py:68
  110.0 1.1 fusion.3
  (25 shorter events, 0.5 us)
Async XLA Ops:
  6.5 41.2 %all-gather.4.cloned.1.call-start = ((), (), s32[]{:S(2)}) async-start(), calls=%async_computation.3 | async-start | bytes 1179648 | tf_op jit(solution)/shard_map/all_gather | solution.py:49
  7.3 52.9 %all-gather.6.cloned.1.call-start = ((), (), s32[]{:S(2)}) async-start(), calls=%async_computation.4 | async-start | bytes 1179648 | tf_op jit(solution)/shard_map/all_gather | solution.py:50
  8.0 75.7 %all-gather.8.cloned.1.call-start = ((), (), s32[]{:S(2)}) async-start(), calls=%async_computation.5 | async-start | bytes 1179648 | tf_op jit(solution)/shard_map/all_gather | solution.py:51
  85.9 17.7 %copy-start = (f32[256,2]{0,1:T(2,128)S(1)}, f32[256,2]{0,1:T(2,128)}, u32[]{:S(2)}) copy-start(f32[256,2]{0,1:T(2,128)} %param.10) | copy-start | bytes 6148
  99.7 9.0 %all-to-all-start.2 = ((bf16[4,256,128]{2,1,0:T(8,128)(2,1)}), bf16[4,256,128]{2,1,0:T(8,128)(2,1)S(1)}, u32[]{:S(2)}, u32[]{:S(2)}) async-start(bf16[4,256,128]{2,1,0:T(8,128)(2,1)} %bitcast.20), calls=%async_computation.2 | async-start | bytes 524288 | tf_op jit(solution)/shard_map/all_to_all | solution.py:65
Sparse Core Ops, SparseCore 0:
  8.9 27.6 all-gather.3
  38.3 21.8 all-gather.5
  61.8 21.8 all-gather.7
